TPU v7x, 32 devices: a whole 2x2x4 slice. The times are simulated.
32 devices in a mesh: ep: 8 (over z, x), tp: 4 (over y, core).
Axes of the slice: x: 2, y: 2, z: 4, core: 2. Of those that a mesh axis runs over, the one named last changes fastest.
Arguments:
- x_mix: bfloat16 [2048, 2048], P('ep'), may hold values from -6 to 6
- mix_gain: float32 [2048], replicated, may hold values from 0.1 to 1.9
- w_query: bfloat16 [2048, 2048], P(None, 'tp'), may hold values from -0.125 to 0.125
- w_key: bfloat16 [2048, 2048], P(None, 'tp'), may hold values from -0.125 to 0.125
- w_value: bfloat16 [2048, 2048], P(None, 'tp'), may hold values from -0.125 to 0.125
- query_gain: float32 [64], replicated, may hold values from 1 to 1.8
- key_gain: float32 [64], replicated, may hold values from 1 to 1.8
- mix_lambda: float32 [16], P('tp'), may hold values from 0.3 to 0.8
- head_gain: float32 [128], replicated, may hold values from 0.1 to 1.9
- w_mix_out: bfloat16 [2048, 2048], P(None, 'tp'), may hold values from -0.125 to 0.125
- x_exp: bfloat16 [1024, 2048], P('ep'), may hold values from -6 to 6
- exp_gain: float32 [2048], replicated, may hold values from 0.1 to 1.9
- routes: int32 [1024, 4], P('ep'), may hold values from 0 to 7, all different within a row; in each aligned block of 128 rows (0 to 127, 128 to 255, ...) at most 96 rows name the same one
- route_weight: float32 [1024, 4], P('ep'), may hold values from 0.1 to 1
- w_gate: bfloat16 [8, 2048, 2048], P('ep', None, 'tp'), may hold values from -0.375 to 0.375
- w_up: bfloat16 [8, 2048, 2048], P('ep', None, 'tp'), may hold values from -0.375 to 0.375
- w_down: bfloat16 [8, 2048, 2048], P('ep', None, 'tp'), may hold values from -0.03125 to 0.03125
Outputs:
- attn_out: bfloat16 [2048, 2048], P('ep', 'tp')
- moe_out: bfloat16 [1024, 2048], P('ep', 'tp')
Inputs may be any that keep to these rules, and one draw needn't show every extreme that they name: `routes`: each row names 4 different experts. In each aligned block of 128 rows (the rows of one index of ep), no expert is named by more than 96 rows, a bound that some block reaches.
All inputs are finite; a program needn't handle non-finite values.
Results may differ from a plain program's by a relative error of at most 0.011.
Values may be sent and summed in bfloat16 or wider, within the bound.
A program may use at most 128 MiB of HBM per device.

v0:
```python
import jax
import jax.numpy as jnp
from jax import lax
from jax.sharding import PartitionSpec as P


def rms_rows(matrix, gain, epsilon):
    wide = matrix.astype(jnp.float32)
    return wide * lax.rsqrt(jnp.mean(wide * wide, axis=-1, keepdims=True) + epsilon) * gain


def slot_ids(chosen_rows, experts, capacity):
    flat_ids = chosen_rows.reshape(-1)
    onehot = (flat_ids[:, None] == lax.iota(jnp.int32, experts)[None, :]).astype(jnp.int32)
    before = jnp.cumsum(onehot, axis=0) - onehot
    position = jnp.sum(before * onehot, axis=1)
    return flat_ids * capacity + position


def attend(
    x_mix, mix_gain, w_query, w_key, w_value, query_gain, key_gain, mix_lambda, head_gain, w_mix_out
):
    row_count = x_mix.shape[0]
    head_size = query_gain.shape[0]
    head_count = w_query.shape[1] // (2 * head_size)
    normed = rms_rows(x_mix, mix_gain, 1e-05).astype(jnp.bfloat16)
    queries = jnp.dot(normed, w_query, preferred_element_type=jnp.float32).reshape(
        row_count, head_count, 2, head_size
    )
    queries = (rms_rows(queries, query_gain, 1e-06) * head_size ** (-0.5)).astype(jnp.bfloat16)
    key_rows = jnp.dot(normed, w_key, preferred_element_type=jnp.float32).reshape(
        row_count, head_count, 2, head_size
    )
    key_rows = (
        rms_rows(key_rows, key_gain, 1e-06)
        .astype(jnp.bfloat16)
        .reshape(row_count, head_count * 2 * head_size)
    )
    values = jnp.dot(normed, w_value, preferred_element_type=jnp.float32).astype(jnp.bfloat16)
    query_pos = lax.axis_index("ep") * row_count + lax.iota(jnp.int32, row_count)
    key_piece = lax.all_gather(key_rows, "ep", axis=0, tiled=True)
    value_piece = lax.all_gather(values, "ep", axis=0, tiled=True)
    piece_rows = key_piece.shape[0]
    key_piece = key_piece.reshape(piece_rows, head_count, 2, head_size)
    value_piece = value_piece.reshape(piece_rows, head_count, 2 * head_size)
    scores = jnp.einsum("qhcd,khcd->cqhk", queries, key_piece, preferred_element_type=jnp.float32)
    key_pos = lax.iota(jnp.int32, piece_rows)
    visible = key_pos[None, :] <= query_pos[:, None]
    weights_exp = jnp.where(visible[None, :, None, :], jnp.exp(scores), 0.0)
    denominator = jnp.sum(weights_exp, axis=-1)
    numerator = jnp.einsum(
        "cqhk,khd->cqhd",
        weights_exp.astype(jnp.bfloat16),
        value_piece,
        preferred_element_type=jnp.float32,
    )
    numerator, denominator = (numerator, denominator)
    head_mix = (
        numerator[0] / denominator[0][..., None]
        - mix_lambda[None, :, None] * numerator[1] / denominator[1][..., None]
    )
    head_rows = (rms_rows(head_mix, head_gain, 1e-05) * 0.8).astype(jnp.bfloat16)
    head_rows = head_rows.reshape(row_count, head_count * 2 * head_size)
    projected = jnp.dot(
        lax.all_gather(head_rows, "tp", axis=1, tiled=True),
        w_mix_out,
        preferred_element_type=jnp.float32,
    )
    return projected.astype(jnp.bfloat16)


def route_experts(x_exp, exp_gain, routes, route_weight, w_gate, w_up, w_down):
    row_count = x_exp.shape[0]
    top_count = routes.shape[1]
    model_width = x_exp.shape[1]
    experts = lax.axis_size("ep")
    capacity = 3 * row_count * top_count // (2 * experts)
    gate_local = w_gate[0]
    up_local = w_up[0]
    down_local = w_down[0]
    local_width = down_local.shape[1]
    normed = rms_rows(x_exp, exp_gain, 1e-05).astype(jnp.bfloat16)
    slot_index = slot_ids(routes, experts, capacity)
    pair_rows = lax.iota(jnp.int32, row_count * top_count) // top_count
    source = jnp.zeros((experts * capacity,), jnp.int32).at[slot_index].set(pair_rows)
    filled = jnp.zeros((experts * capacity,), jnp.bool_).at[slot_index].set(True)
    picked_rows = jnp.where(filled[:, None], normed[source], jnp.zeros((), jnp.bfloat16))
    outgoing = picked_rows.reshape(experts, capacity, model_width)
    incoming = lax.all_to_all(outgoing, "ep", split_axis=0, concat_axis=0, tiled=True)
    item_count = incoming.shape[1]
    flat_rows = incoming.reshape(-1, model_width)
    gate_pre = jnp.dot(flat_rows, gate_local, preferred_element_type=jnp.float32)
    up_pre = jnp.dot(flat_rows, up_local, preferred_element_type=jnp.float32)
    expert_gate_pre = gate_pre
    expert_up_pre = up_pre
    expert_gate_pre = jnp.minimum(expert_gate_pre, 7.0)
    expert_up_pre = jnp.clip(expert_up_pre, -7.0, 7.0)
    hidden = (
        expert_gate_pre * jax.nn.sigmoid(1.702 * expert_gate_pre) * (expert_up_pre + 1.0)
    ).astype(jnp.bfloat16)
    result = jnp.dot(
        lax.all_gather(hidden, "tp", axis=1, tiled=True),
        down_local,
        preferred_element_type=jnp.float32,
    )
    result = result.astype(jnp.bfloat16).reshape(experts, item_count, local_width)
    returned = lax.all_to_all(result, "ep", split_axis=0, concat_axis=0, tiled=True)
    picked = returned.reshape(experts * capacity, local_width)[slot_index]
    picked = picked.reshape(row_count, top_count, local_width).astype(jnp.float32)
    combined = jnp.sum(picked * route_weight[:, :, None], axis=1)
    return combined.astype(jnp.bfloat16)


def body(
    x_mix,
    mix_gain,
    w_query,
    w_key,
    w_value,
    query_gain,
    key_gain,
    mix_lambda,
    head_gain,
    w_mix_out,
    x_exp,
    exp_gain,
    routes,
    route_weight,
    w_gate,
    w_up,
    w_down,
):
    attn_out = attend(
        x_mix,
        mix_gain,
        w_query,
        w_key,
        w_value,
        query_gain,
        key_gain,
        mix_lambda,
        head_gain,
        w_mix_out,
    )
    moe_out = route_experts(x_exp, exp_gain, routes, route_weight, w_gate, w_up, w_down)
    return (attn_out, moe_out)


def solution(mesh):
    return jax.shard_map(
        body,
        mesh=mesh,
        in_specs=(
            P("ep", None),
            P(),
            P(None, "tp"),
            P(None, "tp"),
            P(None, "tp"),
            P(),
            P(),
            P("tp"),
            P(),
            P(None, "tp"),
            P("ep", None),
            P(),
            P("ep", None),
            P("ep", None),
            P("ep", None, "tp"),
            P("ep", None, "tp"),
            P("ep", None, "tp"),
        ),
        out_specs=(P("ep", "tp"), P("ep", "tp")),
        check_vma=False,
    )
```

profile of v0, /device:TPU:0, one launch (start us, length us, event | category | flops | bytes accessed | tf_op | source)
XLA Modules:
  0.0 233.7 jit_solution(14530396072772306226)
XLA Ops:
  7.2 1.6 fusion.4
  8.9 3.5 %fusion.52 = (f32[256,512]{1,0:T(8,128)S(1)}, f32[256,512]{1,0:T(8,128)}) fusion(bf16[2048,512]{1,0:T(8,128)(2,1)} %param.20, bf16[256,2048]{1,0:T(8,128)(2,1)} %param.17, f32[2048]{0:T(1024)} %param.18, f32[256]{0:T(256)S(1)} %add_rsqrt_fusion.3), kind=kOutput, calls=%fused_computation.90 | convolution fusion | flops 539099136 | bytes 4203520 | tf_op jit(solution)/shard_map/dot_general | solution.py:31
  12.7 0.9 mul.194
  13.5 1.2 copy.27
  14.9 1.9 multiply_convert_fusion.2
  17.1 1.1 reduce-window.6
  18.9 2.4 %scatter_custom_fusion.1 = s32[768]{0:T(1024)S(1)} fusion(s32[512]{0:T(512)S(1)} %bitcast.123, s32[512]{0:T(512)S(1)} %add_select_fusion, s32[]{:T(128)} %constant.65.clone.1), kind=kCustom, calls=%fused_computation.76 | custom fusion | bytes 3076 | tf_op jit(solution)/shard_map/scatter | solution.py:85
  21.6 2.4 %scatter_custom_fusion = pred[768]{0:T(1024)(128)(4,1)S(1)} fusion(s32[512]{0:T(512)S(1)} %bitcast.124, pred[512]{0:T(512)(128)(4,1)S(1)} %broadcast.164, pred[]{:T(512)} %constant.25.clone.1), kind=kCustom, calls=%fused_computation.79 | custom fusion | bytes 769 | tf_op jit(solution)/shard_map/scatter | solution.py:86
  24.3 4.3 %gather_fusion = bf16[768,2048]{1,0:T(8,128)(2,1)} fusion(bf16[128,2048]{1,0:T(8,128)(2,1)S(1)} %fusion.25, s32[1024]{0:T(1024)S(1)} %pad_clamp_fusion.1), kind=kCustom, calls=%fused_computation | custom fusion | bytes 6294528 | tf_op jit(solution)/shard_map/gather | solution.py:87
  28.6 3.9 %broadcast_select_fusion = bf16[8,96,2048]{2,1,0:T(8,128)(2,1)} fusion(bf16[8,96,2048]{2,1,0:T(8,128)(2,1)} %bitcast.118, pred[8,96]{1,0:T(8,128)(4,1)S(1)} %broadcast_in_dim.32), kind=kLoop, calls=%fused_computation.9 | loop fusion | flops 1572864 | bytes 6292224 | tf_op jit(solution)/shard_map/jit(_where)/select_n | solution.py:87
  32.5 7.4 %all-to-all-start = ((bf16[8,96,2048]{2,1,0:T(8,128)(2,1)}), bf16[8,96,2048]{2,1,0:T(8,128)(2,1)}, u32[]{:S(2)}, u32[]{:S(2)}) async-start(bf16[8,96,2048]{2,1,0:T(8,128)(2,1)} %broadcast_select_fusion), calls=%async_computation | async-start | bytes 6291456 | tf_op jit(solution)/shard_map/all_to_all | solution.py:89
  40.0 3.0 %convolution_convert_fusion.1 = bf16[256,512]{1,0:T(8,128)(2,1)} fusion(bf16[2048,512]{1,0:T(8,128)(2,1)} %param.21, bf16[256,2048]{1,0:T(8,128)(2,1)S(1)} %copy-done.3, f32[2048]{0:T(1024)S(1)} %copy-done.11, f32[256]{0:T(256)S(1)} %add_rsqrt_fusion.3), kind=kOutput, calls=%fused_computation.30 | convolution fusion | flops 539099136 | bytes 3417088 | tf_op jit(solution)/shard_map/dot_general | solution.py:39
  43.1 93.0 %all-to-all-done = bf16[8,96,2048]{2,1,0:T(8,128)(2,1)} async-done(((bf16[8,96,2048]{2,1,0:T(8,128)(2,1)}), bf16[8,96,2048]{2,1,0:T(8,128)(2,1)}, u32[]{:S(2)}, u32[]{:S(2)}) %all-to-all-start) | async-done | bytes 3145760 | tf_op jit(solution)/shard_map/all_to_all | solution.py:89
  136.1 3.8 %fusion.11 = f32[768,512]{1,0:T(8,128)S(1)} fusion(bf16[768,2048]{1,0:T(8,128)(2,1)} %bitcast.25, bf16[1,2048,512]{2,1,0:T(8,128)(2,1)S(1)} %copy-done), kind=kOutput, calls=%fused_computation.19 | convolution fusion | flops 1610612736 | bytes 6815744 | tf_op jit(solution)/shard_map/dot_general | solution.py:92
  140.0 4.9 %multiply_convert_fusion = bf16[768,512]{1,0:T(8,128)(2,1)} fusion(f32[768,512]{1,0:T(8,128)S(1)} %fusion.11, bf16[768,2048]{1,0:T(8,128)(2,1)} %bitcast.25, bf16[1,2048,512]{2,1,0:T(8,128)(2,1)S(1)} %copy-done.10), kind=kOutput, calls=%fused_computation.24 | convolution fusion | flops 1614544896 | bytes 7602176 | tf_op jit(solution)/shard_map/dot_general | solution.py:93
  145.3 3.5 %multiply_reduce_fusion.1 = (f32[256,4,2]{0,2,1:T(2,128)S(1)}, f32[256,512]{0,1:T(8,128)}) fusion(bf16[2048,512]{1,0:T(8,128)(2,1)} %param.19, bf16[256,2048]{1,0:T(8,128)(2,1)S(1)} %copy-done.3, f32[2048]{0:T(1024)S(1)} %copy-done.11, f32[256]{0:T(256)S(1)} %add_rsqrt_fusion.3), kind=kOutput, calls=%fused_computation.49 | convolution fusion | flops 539228160 | bytes 3687424 | tf_op jit(solution)/shard_map/dot_general | solution.py:27
  148.8 0.3 iota_compare_fusion
  149.1 4.0 %copy.28 = bf16[2048,512]{0,1:T(8,128)(2,1)} copy(bf16[2048,512]{1,0:T(8,128)(2,1)} %all-gather.7.cloned.1.call-done) | data formatting | bytes 4194304 | tf_op jit(solution)/shard_map/all_gather | solution.py:41
  153.1 8.7 %all-gather.5.cloned.1.call-done = bf16[2048,512]{1,0:T(8,128)(2,1)} async-done(((bf16[256,512]{1,0:T(8,128)(2,1)}), bf16[2048,512]{1,0:T(8,128)(2,1)}) %all-gather.5.cloned.1.call-update) | async-done | bytes 2097168 | tf_op jit(solution)/shard_map/all_gather | solution.py:42
  161.9 3.9 %copy.42 = bf16[2048,512]{0,1:T(8,128)(2,1)} copy(bf16[2048,512]{1,0:T(8,128)(2,1)} %all-gather.5.cloned.1.call-done) | data formatting | bytes 4194304 | tf_op jit(solution)/shard_map/reshape | solution.py:45
  165.8 6.7 %fusion = (f32[2,256,4]{1,2,0:T(4,128)S(1)}, bf16[2,256,4,2048]{1,3,2,0:T(8,128)(2,1)S(1)}) fusion(pred[256,2048]{0,1:T(8,128)(4,1)S(1)} %iota_compare_fusion, bf16[2048,4,2,64]{0,3,2,1:T(8,128)(2,1)} %bitcast.120, f32[64]{0:T(128)S(1)} %copy-done.12, f32[256,4,2]{0,2,1:T(2,128)S(1)} %add_rsqrt_fusion, f32[256,512]{0,1:T(8,128)S(1)} %copy-done.13), kind=kOutput, calls=%fused_computation.5 | convolution fusion | flops 549976064 | bytes 11550976 | tf_op jit(solution)/shard_map/qhcd,khcd->cqhk/dot_general | solution.py:46
  172.5 1.3 fusion.20
  174.1 0.9 fusion.33
  175.1 15.4 %all-gather.11.cloned.1.call-done = bf16[768,2048]{1,0:T(8,128)(2,1)} async-done(((bf16[768,512]{1,0:T(8,128)(2,1)}), bf16[768,2048]{1,0:T(8,128)(2,1)}) %all-gather.11.cloned.1.call-update) | async-done | bytes 3145744 | tf_op jit(solution)/shard_map/all_gather | solution.py:102
  190.5 5.2 %fusion.17 = bf16[768,512]{1,0:T(8,128)(2,1)} fusion(bf16[768,2048]{1,0:T(8,128)(2,1)} %all-gather.11.cloned.1.call-done, bf16[1,2048,512]{2,1,0:T(8,128)(2,1)} %param.33), kind=kOutput, calls=%fused_computation.25 | convolution fusion | flops 1611005952 | bytes 6029312 | tf_op jit(solution)/shard_map/dot_general | solution.py:101
  195.7 5.5 %all-to-all-start.1 = ((bf16[8,96,512]{2,1,0:T(8,128)(2,1)}), bf16[8,96,512]{2,1,0:T(8,128)(2,1)S(1)}, u32[]{:S(2)}, u32[]{:S(2)}) async-start(bf16[8,96,512]{2,1,0:T(8,128)(2,1)} %bitcast.122), calls=%async_computation.1 | async-start | bytes 1572864 | tf_op jit(solution)/shard_map/all_to_all | solution.py:107
  201.4 7.9 %all-gather.9.cloned.1.call-done = bf16[256,2048]{0,1:T(8,128)(2,1)} async-done(((bf16[256,512]{0,1:T(8,128)(2,1)}), bf16[256,2048]{0,1:T(8,128)(2,1)}) %all-gather.9.cloned.1.call-update) | async-done | bytes 1048592 | tf_op jit(solution)/shard_map/all_gather | solution.py:65
  209.2 3.3 %convolution_convert_fusion = bf16[256,512]{1,0:T(8,128)(2,1)} fusion(bf16[256,2048]{0,1:T(8,128)(2,1)} %all-gather.9.cloned.1.call-done, bf16[2048,512]{1,0:T(8,128)(2,1)} %param.26), kind=kOutput, calls=%fused_computation.29 | convolution fusion | flops 537001984 | bytes 3407872 | tf_op jit(solution)/shard_map/dot_general | solution.py:64
  212.6 9.2 %all-to-all-done.1 = bf16[8,96,512]{2,1,0:T(8,128)(2,1)S(1)} async-done(((bf16[8,96,512]{2,1,0:T(8,128)(2,1)}), bf16[8,96,512]{2,1,0:T(8,128)(2,1)S(1)}, u32[]{:S(2)}, u32[]{:S(2)}) %all-to-all-start.1) | async-done | bytes 786464 | tf_op jit(solution)/shard_map/all_to_all | solution.py:107
  221.8 2.6 %gather_fusion.1 = bf16[512,512]{1,0:T(8,128)(2,1)} fusion(bf16[768,512]{1,0:T(8,128)(2,1)S(1)} %bitcast.117, s32[1024]{0:T(1024)S(1)} %pad_clamp_fusion), kind=kCustom, calls=%fused_computation.1 | custom fusion | bytes 1050624 | tf_op jit(solution)/shard_map/gather | solution.py:108
  224.4 1.4 reshape.170
  225.8 1.4 multiply_reduce_fusion
  (72 shorter events, 2.8 us)
Async XLA Ops:
  7.2 129.0 %copy-start = (bf16[1,2048,512]{2,1,0:T(8,128)(2,1)S(1)}, bf16[1,2048,512]{2,1,0:T(8,128)(2,1)}, u32[]{:S(2)}) copy-start(bf16[1,2048,512]{2,1,0:T(8,128)(2,1)} %param.31) | copy-start | bytes 6291460
  7.2 141.9 %all-gather.7.cloned.1.call-start = ((), (), s32[]{:S(2)}) async-start(), calls=%async_computation.3 | async-start | bytes 2359296 | tf_op jit(solution)/shard_map/all_gather | solution.py:41
  12.4 2.4 %copy-start.8 = (f32[64]{0:T(128)S(1)}, f32[64]{0:T(128)}, u32[]{:S(2)}) copy-start(f32[64]{0:T(128)} %param.23) | copy-start | bytes 772
  12.6 4.2 %copy-start.5 = (s32[128,4]{0,1:T(4,128)S(1)}, s32[128,4]{0,1:T(4,128)}, u32[]{:S(2)}) copy-start(s32[128,4]{0,1:T(4,128)} %param.29) | copy-start | bytes 6148
  12.6 8.8 %copy-start.2 = (bf16[128,2048]{1,0:T(8,128)(2,1)S(1)}, bf16[128,2048]{1,0:T(8,128)(2,1)}, u32[]{:S(2)}) copy-start(bf16[128,2048]{1,0:T(8,128)(2,1)} %param.27) | copy-start | bytes 1572868
  12.7 11.5 %copy-start.4 = (f32[2048]{0:T(1024)S(1)}, f32[2048]{0:T(1024)}, u32[]{:S(2)}) copy-start(f32[2048]{0:T(1024)} %param.28) | copy-start | bytes 24580
  32.5 7.5 %copy-start.3 = (bf16[256,2048]{1,0:T(8,128)(2,1)S(1)}, bf16[256,2048]{1,0:T(8,128)(2,1)}, u32[]{:S(2)}) copy-start(bf16[256,2048]{1,0:T(8,128)(2,1)} %param.17) | copy-start | bytes 3145732
  32.5 7.5 %copy-start.11 = (f32[2048]{0:T(1024)S(1)}, f32[2048]{0:T(1024)}, u32[]{:S(2)}) copy-start(f32[2048]{0:T(1024)} %param.18) | copy-start | bytes 24580
  32.5 103.6 %all-to-all-start = ((bf16[8,96,2048]{2,1,0:T(8,128)(2,1)}), bf16[8,96,2048]{2,1,0:T(8,128)(2,1)}, u32[]{:S(2)}, u32[]{:S(2)}) async-start(bf16[8,96,2048]{2,1,0:T(8,128)(2,1)} %broadcast_select_fusion), calls=%async_computation | async-start | bytes 6291456 | tf_op jit(solution)/shard_map/all_to_all | solution.py:89
  39.9 121.9 %all-gather.5.cloned.1.call-start = ((), (), s32[]{:S(2)}) async-start(), calls=%async_computation.2 | async-start | bytes 2359296 | tf_op jit(solution)/shard_map/all_gather | solution.py:42
  43.1 147.4 %all-gather.11.cloned.1.call-start = ((), (), s32[]{:S(2)}) async-start(), calls=%async_computation.5 | async-start | bytes 3932160 | tf_op jit(solution)/shard_map/all_gather | solution.py:102
  136.1 3.8 %copy-start.10 = (bf16[1,2048,512]{2,1,0:T(8,128)(2,1)S(1)}, bf16[1,2048,512]{2,1,0:T(8,128)(2,1)}, u32[]{:S(2)}) copy-start(bf16[1,2048,512]{2,1,0:T(8,128)(2,1)} %param.32) | copy-start | bytes 6291460
  140.0 5.2 %copy-start.6 = (f32[4]{0:T(128)S(1)}, f32[4]{0:T(128)}, u32[]{:S(2)}) copy-start(f32[4]{0:T(128)} %param.24) | copy-start | bytes 52
  140.0 5.2 %copy-start.9 = (f32[128]{0:T(128)S(1)}, f32[128]{0:T(128)}, u32[]{:S(2)}) copy-start(f32[128]{0:T(128)} %param.25) | copy-start | bytes 1540
  144.9 64.3 %all-gather.9.cloned.1.call-start = ((), (), s32[]{:S(2)}) async-start(), calls=%async_computation.4 | async-start | bytes 1310720 | tf_op jit(solution)/shard_map/all_gather | solution.py:65
  153.1 12.7 %copy-start.12 = (f32[64]{0:T(128)S(1)}, f32[64]{0:T(128)}, u32[]{:S(2)}) copy-start(f32[64]{0:T(128)} %param.22) | copy-start | bytes 772
  153.1 12.7 %copy-start.13 = (f32[256,512]{0,1:T(8,128)S(1)}, f32[256,512]{0,1:T(8,128)}, u32[]{:S(2)}) copy-start(f32[256,512]{0,1:T(8,128)} %get-tuple-element.11) | copy-start | bytes 1572868
  165.8 6.7 %copy-start.1 = (bf16[2048,512]{0,1:T(8,128)(2,1)S(1)}, bf16[2048,512]{0,1:T(8,128)(2,1)}, u32[]{:S(2)}) copy-start(bf16[2048,512]{0,1:T(8,128)(2,1)} %copy.42) | copy-start | bytes 6291460
  175.0 26.2 %copy-start.7 = (f32[128,4]{0,1:T(4,128)S(1)}, f32[128,4]{0,1:T(4,128)}, u32[]{:S(2)}) copy-start(f32[128,4]{0,1:T(4,128)} %param.30) | copy-start | bytes 6148
  195.7 26.1 %all-to-all-start.1 = ((bf16[8,96,512]{2,1,0:T(8,128)(2,1)}), bf16[8,96,512]{2,1,0:T(8,128)(2,1)S(1)}, u32[]{:S(2)}, u32[]{:S(2)}) async-start(bf16[8,96,512]{2,1,0:T(8,128)(2,1)} %bitcast.122), calls=%async_computation.1 | async-start | bytes 1572864 | tf_op jit(solution)/shard_map/all_to_all | solution.py:107
Sparse Core Ops, SparseCore 0:
  16.9 67.8 all-gather.6
  87.5 74.3 all-gather.4
  163.4 27.0 all-gather.10
  192.5 16.6 all-gather.8
where the time goes:
time: 234 us
  waiting for transfers between devices  134 us (57%)
  matrix products  35.2 us (15%)
  local copies, waits for them, and re-layouts  24.7 us (11%)
  between operations  14.1 us (6%)
  starting transfers between devices  13.3 us (6%)
  other arithmetic  12 us (5%)
    all_to_all x1, waiting for transfers between devices, route_experts(): lax.all_to_all(outgoing, 'ep', split_axis=0, concat_axis=0, tiled=True)  93 us
    all_gather x1, waiting for transfers between devices, route_experts(): lax.all_gather(hidden, 'tp', axis=1, tiled=True)  15.4 us
    all_to_all x1, waiting for transfers between devices, route_experts(): lax.all_to_all(result, 'ep', split_axis=0, concat_axis=0, tiled=True)  9.19 us
    all_gather x1, waiting for transfers between devices, attend(): value_piece = lax.all_gather(values, 'ep', axis=0, tiled=True)  8.72 us
    all_gather x1, waiting for transfers between devices, attend(): lax.all_gather(head_rows, 'tp', axis=1, tiled=True)  7.88 us
    all_to_all x1, starting transfers between devices, route_experts(): lax.all_to_all(outgoing, 'ep', split_axis=0, concat_axis=0, tiled=True)  7.43 us
    dot_general x1, matrix products, attend(): jnp.einsum('qhcd,khcd->cqhk', queries, key_piece, preferred_element_type=...  6.69 us
    all_to_all x1, starting transfers between devices, route_experts(): lax.all_to_all(result, 'ep', split_axis=0, concat_axis=0, tiled=True)  5.51 us
  transfers between devices with their start and end apart: 6, of which 5 were waited for; matrix products, arithmetic and copies ran while one was open for 24% of the time, Pallas kernels for 0%

commit v1 on v0

--- a/solution.py
+++ b/solution.py
@@ -38,8 +38,11 @@
     )
     values = jnp.dot(normed, w_value, preferred_element_type=jnp.float32).astype(jnp.bfloat16)
     query_pos = lax.axis_index("ep") * row_count + lax.iota(jnp.int32, row_count)
-    key_piece = lax.all_gather(key_rows, "ep", axis=0, tiled=True)
-    value_piece = lax.all_gather(values, "ep", axis=0, tiled=True)
+    key_piece, value_piece = jnp.split(
+        lax.all_gather(jnp.concatenate([key_rows, values], axis=1), "ep", axis=0, tiled=True),
+        [key_rows.shape[1]],
+        axis=1,
+    )
     piece_rows = key_piece.shape[0]
     key_piece = key_piece.reshape(piece_rows, head_count, 2, head_size)
     value_piece = value_piece.reshape(piece_rows, head_count, 2 * head_size)

time: 234 us -> 227 us (0.970)
  blocking collectives: 0 us -> 119 us
  waiting for transfers between devices: 134 us -> 18.4 us
  starting transfers between devices: 13.3 us -> 5.81 us
  matrix products: 35.2 us -> 29.1 us
  local copies, waits for them, and re-layouts: 24.7 us -> 29.8 us
    all_to_all x0 -> x1, blocking collectives: none -> 119 us  [route_experts(): lax.all_to_all(outgoing, 'ep', split_axis=0, concat_axis=0, tiled=True)]
    all_to_all x1 -> x0, waiting for transfers between devices: 93 us -> none  [route_experts(): lax.all_to_all(outgoing, 'ep', split_axis=0, concat_axis=0, tiled=True)]
    all_gather x1, waiting for transfers between devices: 15.4 us -> 1.22 us  [route_experts(): lax.all_gather(hidden, 'tp', axis=1, tiled=True)]
    split x0 -> x2, local copies, waits for them, and re-layouts: none -> 8.96 us  [attend(): jnp.split(lax.all_gather(jnp.concatenate([key_rows, values], axis=1), 'ep...]
    all_gather x2 -> x1, waiting for transfers between devices: 8.75 us -> 0.02 us  [attend(): lax.all_gather(jnp.concatenate([key_rows, values], axis=1), 'ep', axis=0,...]
    all_to_all x1 -> x0, starting transfers between devices: 7.43 us -> none  [route_experts(): lax.all_to_all(outgoing, 'ep', split_axis=0, concat_axis=0, tiled=True)]
    all_gather x1 -> x0, local copies, waits for them, and re-layouts: 4 us -> none  [attend(): key_piece = lax.all_gather(key_rows, 'ep', axis=0, tiled=True)]
  transfers between devices with their start and end apart: 6 -> 4, of which waited for: 5 -> 3; matrix products, arithmetic and copies ran while one was open for 24% -> 24% of each run, Pallas kernels for 0% -> 0%
where the time goes in v1:
time: 227 us; the launch traced here: 226 us
  blocking collectives  119 us (52%)
  local copies, waits for them, and re-layouts  29.8 us (13%)
  matrix products  29.1 us (13%)
  waiting for transfers between devices  18.4 us (8%)
  between operations  14.1 us (6%)
  other arithmetic  10.4 us (5%)
  starting transfers between devices  5.81 us (3%)
    all_to_all x1, blocking collectives, route_experts(): lax.all_to_all(outgoing, 'ep', split_axis=0, concat_axis=0, tiled=True)  119 us
    all_to_all x1, waiting for transfers between devices, route_experts(): lax.all_to_all(result, 'ep', split_axis=0, concat_axis=0, tiled=True)  9.09 us
    split x2, local copies, waits for them, and re-layouts, attend(): jnp.split(lax.all_gather(jnp.concatenate([key_rows, values], axis=1), 'ep...  8.96 us
    all_gather x1, waiting for transfers between devices, attend(): lax.all_gather(head_rows, 'tp', axis=1, tiled=True)  7.99 us
    dot_general x1, matrix products, attend(): jnp.einsum('qhcd,khcd->cqhk', queries, key_piece, preferred_element_type=...  6.69 us
    all_to_all x1, starting transfers between devices, route_experts(): lax.all_to_all(result, 'ep', split_axis=0, concat_axis=0, tiled=True)  5.51 us
    dot_general x1, matrix products, route_experts(): jnp.dot(lax.all_gather(hidden, 'tp', axis=1, tiled=True), down_local, pre...  5.25 us
  transfers between devices with their start and end apart: 4, of which 3 were waited for; matrix products, arithmetic and copies ran while one was open for 24% of the time, Pallas kernels for 0%

profile of v1, /device:TPU:0, one launch (start us, length us, event | category | flops | bytes accessed | tf_op | source)
XLA Modules:
  0.0 226.5 jit_solution(13190883813159320639)
XLA Ops:
  7.2 1.6 fusion.4
  8.9 2.8 %convolution_convert_fusion.1 = bf16[256,512]{1,0:T(8,128)(2,1)S(1)} fusion(bf16[2048,512]{1,0:T(8,128)(2,1)} %param.21, bf16[256,2048]{1,0:T(8,128)(2,1)} %param.17, f32[2048]{0:T(1024)} %param.18, f32[256]{0:T(256)S(1)} %add_rsqrt_fusion.3), kind=kOutput, calls=%fused_computation.30 | convolution fusion | flops 539099136 | bytes 3417088 | tf_op jit(solution)/shard_map/dot_general | solution.py:39
  11.8 1.5 fusion.53
  13.6 0.9 mul.193
  14.5 1.3 copy.27
  15.9 1.1 multiply_convert_fusion.2
  17.0 0.9 pad_maximum_fusion
  18.8 1.1 reduce-window.6
  20.3 2.4 %scatter_custom_fusion.1 = s32[768]{0:T(1024)S(1)} fusion(s32[512]{0:T(512)S(1)} %bitcast.125, s32[512]{0:T(512)S(1)} %add_select_fusion, s32[]{:T(128)} %constant.65.clone.1), kind=kCustom, calls=%fused_computation.77 | custom fusion | bytes 3076 | tf_op jit(solution)/shard_map/scatter | solution.py:88
  22.8 2.4 %scatter_custom_fusion = pred[768]{0:T(1024)(128)(4,1)S(1)} fusion(s32[512]{0:T(512)S(1)} %bitcast.126, pred[512]{0:T(512)(128)(4,1)S(1)} %broadcast.164, pred[]{:T(512)} %constant.25.clone.1), kind=kCustom, calls=%fused_computation.80 | custom fusion | bytes 769 | tf_op jit(solution)/shard_map/scatter | solution.py:89
  25.5 4.3 %gather_fusion = bf16[768,2048]{1,0:T(8,128)(2,1)} fusion(bf16[128,2048]{1,0:T(8,128)(2,1)S(1)} %fusion.25, s32[1024]{0:T(1024)S(1)} %pad_clamp_fusion.1), kind=kCustom, calls=%fused_computation | custom fusion | bytes 6294528 | tf_op jit(solution)/shard_map/gather | solution.py:90
  29.8 2.2 broadcast_select_fusion
  32.0 118.9 %all_to_all.10 = bf16[8,96,2048]{2,1,0:T(8,128)(2,1)S(1)} all-to-all(bf16[8,96,2048]{2,1,0:T(8,128)(2,1)S(1)} %broadcast_select_fusion), channel_id=1, replica_groups=mesh['ep'=8,'tp'=4] {'ep'}, dimensions={0} | all-to-all | bytes 6291456 | tf_op jit(solution)/shard_map/all_to_all | solution.py:92
  150.9 1.8 fusion.11
  152.7 3.0 %multiply_convert_fusion = bf16[768,512]{1,0:T(8,128)(2,1)} fusion(f32[768,512]{1,0:T(8,128)S(1)} %fusion.11, bf16[768,2048]{1,0:T(8,128)(2,1)S(1)} %bitcast.120, bf16[1,2048,512]{2,1,0:T(8,128)(2,1)S(1)} %copy-done.12), kind=kOutput, calls=%fused_computation.24 | convolution fusion | flops 1614544896 | bytes 7602176 | tf_op jit(solution)/shard_map/dot_general | solution.py:96
  156.1 3.4 %multiply_reduce_fusion.1 = (f32[256,4,2]{0,2,1:T(2,128)S(1)}, f32[256,512]{0,1:T(8,128)}) fusion(bf16[2048,512]{1,0:T(8,128)(2,1)} %param.19, bf16[256,2048]{1,0:T(8,128)(2,1)S(1)} %copy-done.4, f32[2048]{0:T(1024)S(1)} %copy-done.13, f32[256]{0:T(256)S(1)} %add_rsqrt_fusion.3), kind=kOutput, calls=%fused_computation.50 | convolution fusion | flops 539228160 | bytes 3687424 | tf_op jit(solution)/shard_map/dot_general | solution.py:27
  159.5 0.3 iota_compare_fusion
  159.9 4.9 %fusion.51 = (bf16[2048,512]{1,0:T(8,128)(2,1)}, bf16[2048,512]{1,0:T(8,128)(2,1)}) fusion(bf16[2048,1024]{1,0:T(8,128)(2,1)} %all-gather.4.cloned.1.call-done), kind=kLoop, calls=%fused_computation.90 | loop fusion | bytes 8388608 | tf_op jit(solution)/shard_map/split | solution.py:41
  164.8 4.0 %copy.42 = bf16[2048,512]{0,1:T(8,128)(2,1)} copy(bf16[2048,512]{1,0:T(8,128)(2,1)} %get-tuple-element.5) | data formatting | bytes 4194304 | tf_op jit(solution)/shard_map/reshape | solution.py:48
  168.8 4.0 %copy.28 = bf16[2048,512]{0,1:T(8,128)(2,1)} copy(bf16[2048,512]{1,0:T(8,128)(2,1)} %get-tuple-element.4) | data formatting | bytes 4194304 | tf_op jit(solution)/shard_map/split | solution.py:41
  172.8 6.7 %fusion = (f32[2,256,4]{1,2,0:T(4,128)S(1)}, bf16[2,256,4,2048]{1,3,2,0:T(8,128)(2,1)S(1)}) fusion(pred[256,2048]{0,1:T(8,128)(4,1)S(1)} %iota_compare_fusion, bf16[2048,4,2,64]{0,3,2,1:T(8,128)(2,1)} %bitcast.122, f32[64]{0:T(128)S(1)} %copy-done.14, f32[256,4,2]{0,2,1:T(2,128)S(1)} %add_rsqrt_fusion, f32[256,512]{0,1:T(8,128)S(1)} %copy-done.15), kind=kOutput, calls=%fused_computation.5 | convolution fusion | flops 549976064 | bytes 11550976 | tf_op jit(solution)/shard_map/qhcd,khcd->cqhk/dot_general | solution.py:49
  179.6 1.3 fusion.20
  181.1 0.9 fusion.33
  182.1 1.2 all-gather.8.cloned.1.call-done
  183.3 5.2 %fusion.17 = bf16[768,512]{1,0:T(8,128)(2,1)} fusion(bf16[768,2048]{1,0:T(8,128)(2,1)} %all-gather.8.cloned.1.call-done, bf16[1,2048,512]{2,1,0:T(8,128)(2,1)} %param.33), kind=kOutput, calls=%fused_computation.25 | convolution fusion | flops 1611005952 | bytes 6029312 | tf_op jit(solution)/shard_map/dot_general | solution.py:104
  188.5 5.5 %all-to-all-start.1 = ((bf16[8,96,512]{2,1,0:T(8,128)(2,1)}), bf16[8,96,512]{2,1,0:T(8,128)(2,1)S(1)}, u32[]{:S(2)}, u32[]{:S(2)}) async-start(bf16[8,96,512]{2,1,0:T(8,128)(2,1)} %bitcast.124), calls=%async_computation.1 | async-start | bytes 1572864 | tf_op jit(solution)/shard_map/all_to_all | solution.py:110
  194.2 8.0 %all-gather.6.cloned.1.call-done = bf16[256,2048]{0,1:T(8,128)(2,1)} async-done(((bf16[256,512]{0,1:T(8,128)(2,1)}), bf16[256,2048]{0,1:T(8,128)(2,1)}) %all-gather.6.cloned.1.call-update) | async-done | bytes 1048592 | tf_op jit(solution)/shard_map/all_gather | solution.py:68
  202.2 3.3 %convolution_convert_fusion = bf16[256,512]{1,0:T(8,128)(2,1)} fusion(bf16[256,2048]{0,1:T(8,128)(2,1)} %all-gather.6.cloned.1.call-done, bf16[2048,512]{1,0:T(8,128)(2,1)} %param.26), kind=kOutput, calls=%fused_computation.29 | convolution fusion | flops 537001984 | bytes 3407872 | tf_op jit(solution)/shard_map/dot_general | solution.py:67
  205.5 9.1 %all-to-all-done.1 = bf16[8,96,512]{2,1,0:T(8,128)(2,1)S(1)} async-done(((bf16[8,96,512]{2,1,0:T(8,128)(2,1)}), bf16[8,96,512]{2,1,0:T(8,128)(2,1)S(1)}, u32[]{:S(2)}, u32[]{:S(2)}) %all-to-all-start.1) | async-done | bytes 786464 | tf_op jit(solution)/shard_map/all_to_all | solution.py:110
  214.6 2.6 %gather_fusion.1 = bf16[512,512]{1,0:T(8,128)(2,1)} fusion(bf16[768,512]{1,0:T(8,128)(2,1)S(1)} %bitcast.117, s32[1024]{0:T(1024)S(1)} %pad_clamp_fusion), kind=kCustom, calls=%fused_computation.1 | custom fusion | bytes 1050624 | tf_op jit(solution)/shard_map/gather | solution.py:111
  217.2 1.4 reshape.170
  218.6 1.4 multiply_reduce_fusion
  (74 shorter events, 2.7 us)
Async XLA Ops:
  7.2 143.7 %copy-start = (bf16[1,2048,512]{2,1,0:T(8,128)(2,1)S(1)}, bf16[1,2048,512]{2,1,0:T(8,128)(2,1)}, u32[]{:S(2)}) copy-start(bf16[1,2048,512]{2,1,0:T(8,128)(2,1)} %param.31) | copy-start | bytes 6291460
  7.2 152.7 %all-gather.4.cloned.1.call-start = ((), (), s32[]{:S(2)}) async-start(), calls=%async_computation.2 | async-start | bytes 4718592 | tf_op jit(solution)/shard_map/all_gather | solution.py:42
  8.9 2.9 %copy-start.3 = (bf16[256,2048]{1,0:T(8,128)(2,1)S(1)}, bf16[256,2048]{1,0:T(8,128)(2,1)}, u32[]{:S(2)}) copy-start(bf16[256,2048]{1,0:T(8,128)(2,1)} %param.17) | copy-start | bytes 3145732
  8.9 2.9 %copy-start.11 = (bf16[2048,512]{1,0:T(8,128)(2,1)S(1)}, bf16[2048,512]{1,0:T(8,128)(2,1)}, u32[]{:S(2)}) copy-start(bf16[2048,512]{1,0:T(8,128)(2,1)} %param.20) | copy-start | bytes 6291460
  8.9 2.9 %copy-start.13 = (f32[2048]{0:T(1024)S(1)}, f32[2048]{0:T(1024)}, u32[]{:S(2)}) copy-start(f32[2048]{0:T(1024)} %param.18) | copy-start | bytes 24580
  13.3 2.4 %copy-start.9 = (f32[64]{0:T(128)S(1)}, f32[64]{0:T(128)}, u32[]{:S(2)}) copy-start(f32[64]{0:T(128)} %param.23) | copy-start | bytes 772
  14.5 3.5 %copy-start.6 = (s32[128,4]{0,1:T(4,128)S(1)}, s32[128,4]{0,1:T(4,128)}, u32[]{:S(2)}) copy-start(s32[128,4]{0,1:T(4,128)} %param.29) | copy-start | bytes 6148
  14.5 3.9 %copy-start.2 = (bf16[128,2048]{1,0:T(8,128)(2,1)S(1)}, bf16[128,2048]{1,0:T(8,128)(2,1)}, u32[]{:S(2)}) copy-start(bf16[128,2048]{1,0:T(8,128)(2,1)} %param.27) | copy-start | bytes 1572868
  15.8 9.5 %copy-start.5 = (f32[2048]{0:T(1024)S(1)}, f32[2048]{0:T(1024)}, u32[]{:S(2)}) copy-start(f32[2048]{0:T(1024)} %param.28) | copy-start | bytes 24580
  17.9 165.4 %all-gather.8.cloned.1.call-start = ((), (), s32[]{:S(2)}) async-start(), calls=%async_computation.4 | async-start | bytes 3932160 | tf_op jit(solution)/shard_map/all_gather | solution.py:105
  150.9 1.8 copy-start.12
  152.7 3.3 %copy-start.7 = (f32[4]{0:T(128)S(1)}, f32[4]{0:T(128)}, u32[]{:S(2)}) copy-start(f32[4]{0:T(128)} %param.24) | copy-start | bytes 52
  152.7 3.3 %copy-start.10 = (f32[128]{0:T(128)S(1)}, f32[128]{0:T(128)}, u32[]{:S(2)}) copy-start(f32[128]{0:T(128)} %param.25) | copy-start | bytes 1540
  152.7 3.4 %copy-start.4 = (bf16[256,2048]{1,0:T(8,128)(2,1)S(1)}, bf16[256,2048]{1,0:T(8,128)(2,1)}, u32[]{:S(2)}) copy-start(bf16[256,2048]{1,0:T(8,128)(2,1)} %param.17) | copy-start | bytes 3145732
  155.7 46.4 %all-gather.6.cloned.1.call-start = ((), (), s32[]{:S(2)}) async-start(), calls=%async_computation.3 | async-start | bytes 1310720 | tf_op jit(solution)/shard_map/all_gather | solution.py:68
  168.8 4.0 %copy-start.14 = (f32[64]{0:T(128)S(1)}, f32[64]{0:T(128)}, u32[]{:S(2)}) copy-start(f32[64]{0:T(128)} %param.22) | copy-start | bytes 772
  168.8 4.0 %copy-start.15 = (f32[256,512]{0,1:T(8,128)S(1)}, f32[256,512]{0,1:T(8,128)}, u32[]{:S(2)}) copy-start(f32[256,512]{0,1:T(8,128)} %get-tuple-element.13) | copy-start | bytes 1572868
  172.8 6.7 %copy-start.1 = (bf16[2048,512]{0,1:T(8,128)(2,1)S(1)}, bf16[2048,512]{0,1:T(8,128)(2,1)}, u32[]{:S(2)}) copy-start(bf16[2048,512]{0,1:T(8,128)(2,1)} %copy.42) | copy-start | bytes 6291460
  182.1 12.0 %copy-start.8 = (f32[128,4]{0,1:T(4,128)S(1)}, f32[128,4]{0,1:T(4,128)}, u32[]{:S(2)}) copy-start(f32[128,4]{0,1:T(4,128)} %param.30) | copy-start | bytes 6148
  188.5 26.1 %all-to-all-start.1 = ((bf16[8,96,512]{2,1,0:T(8,128)(2,1)}), bf16[8,96,512]{2,1,0:T(8,128)(2,1)S(1)}, u32[]{:S(2)}, u32[]{:S(2)}) async-start(bf16[8,96,512]{2,1,0:T(8,128)(2,1)} %bitcast.124), calls=%async_computation.1 | async-start | bytes 1572864 | tf_op jit(solution)/shard_map/all_to_all | solution.py:110
Sparse Core Ops, SparseCore 0:
  18.0 123.4 all-gather.3
  155.9 27.3 all-gather.7
  185.4 16.6 all-gather.5
